TPU v7x, 32 devices: a whole 2x2x4 slice. The times are simulated.
32 devices in a mesh: ep: 16 (over z, y, x), tp: 2 (over core).
Axes of the slice: x: 2, y: 2, z: 4, core: 2. Of those that a mesh axis runs over, the one named last changes fastest.
Arguments:
- tokens: bfloat16 [512, 2048], P('ep'), may hold values from -6 to 6
- mix_gain: float32 [2048], replicated, may hold values from 0.1 to 1.9
- w_query: bfloat16 [2048, 512], P('ep', 'tp'), may hold values from -0.125 to 0.125
- w_key: bfloat16 [2048, 512], P('ep', 'tp'), may hold values from -0.125 to 0.125
- w_value: bfloat16 [2048, 512], P('ep', 'tp'), may hold values from -0.125 to 0.125
- w_outgate: bfloat16 [2048, 512], P('ep', 'tp'), may hold values from -0.125 to 0.125
- w_igate: bfloat16 [2048, 8], P('ep', 'tp'), may hold values from -0.125 to 0.125
- w_fgate: bfloat16 [2048, 8], P('ep', 'tp'), may hold values from -0.125 to 0.125
- igate_bias: float32 [8], P('tp'), may hold values from -2 to 1
- fgate_bias: float32 [8], P('tp'), may hold values from 0 to 4
- head_gain: float32 [512], P('tp'), may hold values from 0.1 to 1.9
- w_out: bfloat16 [512, 2048], P('tp', 'ep'), may hold values from -0.25 to 0.25
- state_matrix: float32 [512, 8, 64, 64], P('ep', 'tp'), may hold values from -2.4 to 2.4
- state_norm: float32 [512, 8, 64], P('ep', 'tp'), may hold values from -2.4 to 2.4
- state_max: float32 [512, 8], P('ep', 'tp'), may hold values from -4 to 4
- ffn_gain: float32 [2048], replicated, may hold values from 0.1 to 1.9
- w_expert_gate: bfloat16 [16, 2048, 1408], P('ep', None, 'tp'), may hold values from -0.125 to 0.125
- w_expert_up: bfloat16 [16, 2048, 1408], P('ep', None, 'tp'), may hold values from -0.125 to 0.125
- w_expert_down: bfloat16 [16, 1408, 2048], P('ep', 'tp'), may hold values from -0.15625 to 0.15625
- routes: int32 [512, 3], P('ep'), may hold values from 0 to 15, all different within a row; in each aligned block of 32 rows (0 to 31, 32 to 63, ...) at most 12 rows name the same one
- route_weights: float32 [512, 3], P('ep'), may hold values from 0.2 to 1
Outputs:
- mixed: bfloat16 [512, 2048], P('ep')
- new_matrix: float32 [512, 8, 64, 64], P('ep', 'tp')
- new_norm: float32 [512, 8, 64], P('ep', 'tp')
- new_max: float32 [512, 8], P('ep', 'tp')
Inputs may be any that keep to these rules, and one draw needn't show every extreme that they name: `routes`: each row names 3 different experts. Among the rows of one device, no expert is named by more than 12 rows, a bound that some block reaches.
All inputs are finite; a program needn't handle non-finite values.
Results may differ from a plain program's by a relative error of at most 0.017.
Values may be sent and summed in bfloat16 or wider, within the bound.
No kernel may reach another device: no remote copies, remote signals or barrier semaphores. Data moves between devices by JAX's collectives and lax.ppermute only.
A program may use at most 128 MiB of HBM per device.

v0:
```python
import jax
import jax.numpy as jnp
from jax import lax
from jax.sharding import PartitionSpec as P


def rms_scale(values_in, gain_vec):
    widened = values_in.astype(jnp.float32)
    return (
        widened * lax.rsqrt(jnp.mean(widened * widened, axis=-1, keepdims=True) + 1e-06) * gain_vec
    )


def memory_cell(
    query,
    key_row,
    value_row,
    outgate,
    input_pre,
    forget_pre,
    head_gain,
    state_matrix,
    state_norm,
    state_max,
):
    seq_rows, head_count = input_pre.shape
    head_size = query.shape[1] // head_count
    query_heads = query.astype(jnp.float32).reshape(seq_rows, head_count, head_size)
    key_heads = key_row.astype(jnp.float32).reshape(
        seq_rows, head_count, head_size
    ) * head_size ** (-0.5)
    value_heads = value_row.astype(jnp.float32).reshape(seq_rows, head_count, head_size)
    log_forget = jax.nn.log_sigmoid(forget_pre)
    new_max = jnp.maximum(log_forget + state_max, input_pre)
    keep_old = jnp.exp(log_forget + state_max - new_max)
    keep_new = jnp.exp(input_pre - new_max)
    new_matrix = (
        keep_old[:, :, None, None] * state_matrix
        + keep_new[:, :, None, None] * value_heads[:, :, :, None] * key_heads[:, :, None, :]
    )
    new_norm = keep_old[:, :, None] * state_norm + keep_new[:, :, None] * key_heads
    numerator = jnp.einsum(
        "bhvd,bhd->bhv", new_matrix, query_heads, precision=lax.Precision.HIGHEST
    )
    denominator = jnp.sum(new_norm * query_heads, axis=-1)
    cell_read = numerator / jnp.maximum(jnp.abs(denominator), jnp.exp(-new_max))[:, :, None]
    centered = cell_read - jnp.mean(cell_read, axis=-1, keepdims=True)
    variance = jnp.mean(centered * centered, axis=-1, keepdims=True)
    scaled_cell = (centered * lax.rsqrt(variance + 1e-06)).reshape(seq_rows, head_count * head_size)
    cell_out = (scaled_cell * head_gain * jax.nn.sigmoid(outgate.astype(jnp.float32))).astype(
        jnp.bfloat16
    )
    return (cell_out, new_matrix, new_norm, new_max)


def body(
    tokens,
    mix_gain,
    w_query,
    w_key,
    w_value,
    w_outgate,
    w_igate,
    w_fgate,
    igate_bias,
    fgate_bias,
    head_gain,
    w_out,
    state_matrix,
    state_norm,
    state_max,
    ffn_gain,
    w_expert_gate,
    w_expert_up,
    w_expert_down,
    routes,
    route_weights,
):
    seq_rows, width = tokens.shape
    normed = rms_scale(tokens, mix_gain).astype(jnp.bfloat16)
    weight_list = (w_query, w_key, w_value, w_outgate, w_igate, w_fgate)
    spread = lax.all_to_all(normed, "ep", split_axis=1, concat_axis=0, tiled=True)
    joined = jnp.concatenate(weight_list, axis=1)
    summed = lax.psum_scatter(
        jnp.dot(spread, joined, preferred_element_type=jnp.float32),
        "ep",
        scatter_dimension=0,
        tiled=True,
    )
    bounds = [0]
    for weight in weight_list:
        bounds.append(bounds[-1] + weight.shape[1])
    projected = tuple(
        (summed[:, bounds[index] : bounds[index + 1]] for index in range(len(weight_list)))
    )
    query = projected[0].astype(jnp.bfloat16)
    key_row = projected[1].astype(jnp.bfloat16)
    value_row = projected[2].astype(jnp.bfloat16)
    outgate = projected[3].astype(jnp.bfloat16)
    input_pre = projected[4] + igate_bias
    forget_pre = projected[5] + fgate_bias
    cell_out, new_matrix, new_norm, new_max = memory_cell(
        query,
        key_row,
        value_row,
        outgate,
        input_pre,
        forget_pre,
        head_gain,
        state_matrix,
        state_norm,
        state_max,
    )
    partial_out = jnp.dot(
        cell_out,
        lax.all_gather(w_out, "ep", axis=1, tiled=True),
        preferred_element_type=jnp.float32,
    )
    attended = lax.psum(partial_out.astype(jnp.bfloat16), "tp").astype(jnp.float32)
    resid = (tokens.astype(jnp.float32) + attended).astype(jnp.bfloat16)
    normed_two = rms_scale(resid, ffn_gain).astype(jnp.bfloat16)
    ep_count = lax.axis_size("ep")
    local_experts = w_expert_gate.shape[0]
    expert_total = local_experts * ep_count
    top_count = routes.shape[1]
    capacity = max(2, 2 * seq_rows * top_count // expert_total)
    flat_routes = routes.reshape(-1)
    onehot = (flat_routes[:, None] == jnp.arange(expert_total, dtype=jnp.int32)[None, :]).astype(
        jnp.int32
    )
    earlier = jnp.cumsum(onehot, axis=0, dtype=jnp.int32) - onehot
    slots = jnp.sum(onehot * earlier, axis=1, dtype=jnp.int32)
    targets = flat_routes * capacity + slots
    dispatch = (
        targets[:, None] == jnp.arange(expert_total * capacity, dtype=jnp.int32)[None, :]
    ).astype(jnp.bfloat16)
    route_rows = jnp.repeat(normed_two, top_count, axis=0)
    outgoing = jnp.einsum(
        "rs,rd->sd", dispatch, route_rows, preferred_element_type=jnp.float32
    ).astype(jnp.bfloat16)
    outgoing = outgoing.reshape(expert_total, capacity, width)
    received = lax.all_to_all(outgoing, "ep", split_axis=0, concat_axis=0, tiled=True)
    slot_count = received.shape[1]
    regrouped = received.reshape(ep_count, local_experts, slot_count, width)
    gate_pre = jnp.einsum(
        "nxcd,xdf->nxcf", regrouped, w_expert_gate, preferred_element_type=jnp.float32
    )
    up_pre = jnp.einsum(
        "nxcd,xdf->nxcf", regrouped, w_expert_up, preferred_element_type=jnp.float32
    )
    hidden = (jax.nn.silu(gate_pre) * up_pre).astype(jnp.bfloat16)
    partial_down = jnp.einsum(
        "nxcf,xfd->nxcd", hidden, w_expert_down, preferred_element_type=jnp.float32
    )
    expert_sum = lax.psum(partial_down.astype(jnp.bfloat16), "tp")
    finished = expert_sum.reshape(ep_count * local_experts, slot_count, width)
    returned = lax.all_to_all(finished, "ep", split_axis=0, concat_axis=0, tiled=True)
    picked = jnp.dot(
        dispatch,
        returned.reshape(expert_total * capacity, width),
        preferred_element_type=jnp.float32,
    )
    weighted = jnp.sum(
        picked.reshape(seq_rows, top_count, width) * route_weights[:, :, None], axis=1
    )
    mixed = (resid.astype(jnp.float32) + weighted).astype(jnp.bfloat16)
    return (mixed, new_matrix, new_norm, new_max)


def solution(mesh):
    placed = (
        P("ep", None),
        P(),
        P("ep", "tp"),
        P("ep", "tp"),
        P("ep", "tp"),
        P("ep", "tp"),
        P("ep", "tp"),
        P("ep", "tp"),
        P("tp"),
        P("tp"),
        P("tp"),
        P("tp", "ep"),
        P("ep", "tp", None, None),
        P("ep", "tp", None),
        P("ep", "tp"),
        P(),
        P("ep", None, "tp"),
        P("ep", None, "tp"),
        P("ep", "tp", None),
        P("ep", None),
        P("ep", None),
    )
    return jax.shard_map(
        body,
        mesh=mesh,
        in_specs=placed,
        out_specs=(P("ep", None), P("ep", "tp", None, None), P("ep", "tp", None), P("ep", "tp")),
        check_vma=False,
    )
```

profile of v0, /device:TPU:8, one launch (start us, length us, event | category | flops | bytes accessed | tf_op | source)
XLA Modules:
  0.0 342.0 jit_solution(8380659892496630698)
XLA Ops:
  7.2 1.2 fusion.36
  8.4 1.7 copy_bitcast_fusion
  10.1 7.2 %all-to-all-start = ((bf16[32,16,128]{2,0,1:T(8,128)(2,1)}), bf16[32,16,128]{2,0,1:T(8,128)(2,1)S(1)}, u32[]{:S(2)}, u32[]{:S(2)}) async-start(bf16[32,16,128]{2,0,1:T(8,128)(2,1)} %copy_bitcast_fusion), calls=%async_computation | async-start | bytes 262144 | tf_op jit(solution)/shard_map/all_to_all | solution.py:82
  17.3 0.8 copy.58
  18.1 0.8 copy.59
  19.0 1.1 concatenate.3
  20.0 3.9 %all-to-all-done = bf16[32,16,128]{2,0,1:T(8,128)(2,1)S(1)} async-done(((bf16[32,16,128]{2,0,1:T(8,128)(2,1)}), bf16[32,16,128]{2,0,1:T(8,128)(2,1)S(1)}, u32[]{:S(2)}, u32[]{:S(2)}) %all-to-all-start) | async-done | bytes 131104 | tf_op jit(solution)/shard_map/all_to_all | solution.py:82
  23.9 1.9 fusion.62
  25.8 0.7 all-gather.2.cloned.1.call-update
  26.8 0.1 eq.50
  27.0 0.1 reduce_window_sum.11
  27.1 0.2 select_reduce_fusion
  27.3 125.7 %reduce-scatter.2.cloned.1.call-done = f32[32,1032]{1,0:T(8,128)} async-done(((f32[512,1032]{1,0:T(8,128)}), f32[32,1032]{1,0:T(8,128)}) %reduce-scatter.2.cloned.1.call-update) | async-done | bytes 132112 | tf_op jit(solution)/shard_map/reduce_scatter | solution.py:84
  153.0 0.9 convert.9
  154.1 0.1 reshape.171
  154.4 0.9 broadcast_multiply_fusion.3
  155.3 0.8 subtract_exponential_fusion.1
  156.1 0.8 multiply_reduce_fusion.1
  156.9 3.8 %multiply_add_fusion = f32[32,4,64,64]{3,2,1,0:T(8,128)S(1)} fusion(f32[32,4,64,64]{3,2,1,0:T(8,128)} %param.33, f32[32,4,64]{2,1,0:T(4,128)S(1)} %get-tuple-element.30, f32[32,4,64]{2,1,0:T(4,128)S(1)} %get-tuple-element.31, f32[32,4]{1,0:T(8,128)S(1)} %subtract_exponential_fusion.1), kind=kLoop, calls=%fused_computation | loop fusion | flops 1572864 | bytes 4260352 | tf_op jit(solution)/shard_map/add | solution.py:38
  160.7 2.0 copy-done.1
  162.7 3.4 fusion.63
  166.1 0.2 fusion.59
  166.3 0.2 multiply_reduce_fusion
  166.5 0.1 subtract_multiply_fusion
  166.6 0.1 reshape.152
  166.7 39.0 %all-gather.2.cloned.1.call-done = bf16[256,2048]{1,0:T(8,128)(2,1)} async-done(((bf16[256,128]{1,0:T(8,128)(2,1)}), bf16[256,2048]{1,0:T(8,128)(2,1)}) %all-gather.2.cloned.1.call-update) | async-done | bytes 1048592 | tf_op jit(solution)/shard_map/all_gather | solution.py:116
  205.7 2.2 convolution_convert_fusion.1
  207.9 0.5 multiply_add_fusion.3
  208.4 18.1 %all-reduce.3.cloned.1.call-done = bf16[32,2048]{1,0:T(8,128)(2,1)} async-done(((bf16[32,2048]{1,0:T(8,128)(2,1)}), bf16[32,2048]{1,0:T(8,128)(2,1)}) %all-reduce.3.cloned.1.call-update) | async-done | bytes 131088 | tf_op jit(solution)/shard_map/psum | solution.py:119
  226.5 1.1 fusion.40
  227.6 1.0 fusion.42
  228.6 0.2 broadcast_in_dim.2
  228.8 1.1 reshape.153
  229.9 2.4 convolution_convert_fusion
  232.3 2.1 reshape.154
  234.4 33.1 %all_to_all.29 = bf16[16,12,2048]{2,1,0:T(8,128)(2,1)S(1)} all-to-all(bf16[16,12,2048]{2,1,0:T(8,128)(2,1)} %reshape.154), channel_id=1, replica_groups=mesh['ep'=16,'tp'=2] {'ep'}, dimensions={0} | all-to-all | bytes 1572864 | tf_op jit(solution)/shard_map/all_to_all | solution.py:142
  267.5 1.0 copy-done.4
  268.5 3.8 %fusion.9 = f32[16,1,12,704]{3,0,2,1:T(8,128)} fusion(bf16[1,2048,704]{1,2,0:T(8,128)(2,1)} %param.37, bf16[16,12,2048]{2,1,0:T(8,128)(2,1)S(1)} %all_to_all.29), kind=kOutput, calls=%fused_computation.11 | convolution fusion | flops 553648128 | bytes 4210688 | tf_op jit(solution)/shard_map/nxcd,xdf->nxcf/dot_general | solution.py:145
  272.3 5.2 %fusion.6 = bf16[16,12,2048]{2,0,1:T(8,128)(2,1)} fusion(bf16[1,704,2048]{2,1,0:T(8,128)(2,1)S(1)} %copy-done, bf16[1,2048,704]{1,2,0:T(8,128)(2,1)} %param.38, f32[16,1,12,704]{3,0,2,1:T(8,128)} %fusion.9, bf16[16,12,2048]{2,1,0:T(8,128)(2,1)} %copy-done.4), kind=kOutput, calls=%fused_computation.7 | convolution fusion | flops 1108500480 | bytes 7880704 | tf_op jit(solution)/shard_map/nxcf,xfd->nxcd/dot_general | solution.py:152
  277.6 17.9 %all-reduce.5.cloned.1.call-done = bf16[16,12,2048]{2,0,1:T(8,128)(2,1)} async-done(((bf16[16,12,2048]{2,0,1:T(8,128)(2,1)}), bf16[16,12,2048]{2,0,1:T(8,128)(2,1)}) %all-reduce.5.cloned.1.call-update) | async-done | bytes 786448 | tf_op jit(solution)/shard_map/psum | solution.py:155
  295.5 2.6 copy.65
  298.1 7.1 %all-to-all-start.2 = ((bf16[16,12,2048]{2,1,0:T(8,128)(2,1)}), bf16[16,12,2048]{2,1,0:T(8,128)(2,1)}, u32[]{:S(2)}, u32[]{:S(2)}) async-start(bf16[16,12,2048]{2,1,0:T(8,128)(2,1)} %copy.65), calls=%async_computation.3 | async-start | bytes 2097152 | tf_op jit(solution)/shard_map/all_to_all | solution.py:157
  305.2 0.1 reduce_sum.70
  305.4 0.7 copy.66
  306.0 25.1 %all-to-all-done.2 = bf16[16,12,2048]{2,1,0:T(8,128)(2,1)} async-done(((bf16[16,12,2048]{2,1,0:T(8,128)(2,1)}), bf16[16,12,2048]{2,1,0:T(8,128)(2,1)}, u32[]{:S(2)}, u32[]{:S(2)}) %all-to-all-start.2) | async-done | bytes 786464 | tf_op jit(solution)/shard_map/all_to_all | solution.py:157
  331.1 2.1 reshape.169
  333.2 1.5 fusion.18
  334.7 0.7 fusion.43
  (51 shorter events, 0.9 us)
Async XLA Ops:
  7.2 265.2 %copy-start = (bf16[1,704,2048]{2,1,0:T(8,128)(2,1)S(1)}, bf16[1,704,2048]{2,1,0:T(8,128)(2,1)}, u32[]{:S(2)}) copy-start(bf16[1,704,2048]{2,1,0:T(8,128)(2,1)} %param.39) | copy-start | bytes 8650756
  10.1 13.8 %all-to-all-start = ((bf16[32,16,128]{2,0,1:T(8,128)(2,1)}), bf16[32,16,128]{2,0,1:T(8,128)(2,1)S(1)}, u32[]{:S(2)}, u32[]{:S(2)}) async-start(bf16[32,16,128]{2,0,1:T(8,128)(2,1)} %copy_bitcast_fusion), calls=%async_computation | async-start | bytes 262144 | tf_op jit(solution)/shard_map/all_to_all | solution.py:82
  17.3 135.7 %reduce-scatter.2.cloned.1.call-start = ((), (), s32[]{:S(2)}) async-start(), calls=%async_computation.4 | async-start | bytes 2506752 | tf_op jit(solution)/shard_map/reduce_scatter | solution.py:84
  18.9 7.6 %copy-start.13 = (f32[32,4]{0,1:T(4,128)S(1)}, f32[32,4]{0,1:T(4,128)}, u32[]{:S(2)}) copy-start(f32[32,4]{0,1:T(4,128)} %param.35) | copy-start | bytes 1540
  18.9 7.7 %copy-start.7 = (s32[32,3]{0,1:T(4,128)S(1)}, s32[32,3]{0,1:T(4,128)}, u32[]{:S(2)}) copy-start(s32[32,3]{0,1:T(4,128)} %param.40) | copy-start | bytes 1156
  23.9 130.5 %copy-start.10 = (f32[4]{0:T(128)S(1)}, f32[4]{0:T(128)}, u32[]{:S(2)}) copy-start(f32[4]{0:T(128)} %param.30) | copy-start | bytes 52
  23.9 130.5 %copy-start.15 = (f32[4]{0:T(128)S(1)}, f32[4]{0:T(128)}, u32[]{:S(2)}) copy-start(f32[4]{0:T(128)} %param.29) | copy-start | bytes 52
  23.9 132.2 %copy-start.5 = (f32[32,4,64]{2,1,0:T(4,128)S(1)}, f32[32,4,64]{2,1,0:T(4,128)}, u32[]{:S(2)}) copy-start(f32[32,4,64]{2,1,0:T(4,128)} %param.34) | copy-start | bytes 98308
  25.8 179.9 %all-gather.2.cloned.1.call-start = ((), (), s32[]{:S(2)}) async-start(), calls=%async_computation.5 | async-start | bytes 1114112 | tf_op jit(solution)/shard_map/all_gather | solution.py:116
  26.5 200.0 %all-reduce.3.cloned.1.call-start = ((), (), s32[]{:S(2)}) async-start(), calls=%async_computation.6 | async-start | bytes 262144 | tf_op jit(solution)/shard_map/psum | solution.py:119
  27.3 180.6 %copy-start.11 = (s32[96]{0:T(128)}, s32[96]{0:T(128)S(1)}, u32[]{:S(2)}) copy-start(s32[96]{0:T(128)S(1)} %select_reduce_fusion) | copy-start | bytes 1156
  160.7 2.0 copy-start.1
  162.7 43.0 %copy-start.14 = (f32[256]{0:T(256)S(1)}, f32[256]{0:T(256)}, u32[]{:S(2)}) copy-start(f32[256]{0:T(256)} %param.31) | copy-start | bytes 3076
  162.7 63.8 %copy-start.2 = (bf16[32,2048]{1,0:T(8,128)(2,1)S(1)}, bf16[32,2048]{1,0:T(8,128)(2,1)}, u32[]{:S(2)}) copy-start(bf16[32,2048]{1,0:T(8,128)(2,1)} %param.21) | copy-start | bytes 393220
  162.7 64.9 %copy-start.6 = (f32[2048]{0:T(1024)S(1)}, f32[2048]{0:T(1024)}, u32[]{:S(2)}) copy-start(f32[2048]{0:T(1024)} %param.36) | copy-start | bytes 24580
  207.9 87.6 %all-reduce.5.cloned.1.call-start = ((), (), s32[]{:S(2)}) async-start(), calls=%async_computation.7 | async-start | bytes 1572864 | tf_op jit(solution)/shard_map/psum | solution.py:155
  267.5 1.0 copy-start.4
  277.5 27.7 %copy-start.12 = (s32[96]{0:T(128)S(1)}, s32[96]{0:T(128)}, u32[]{:S(2)}) copy-start(s32[96]{0:T(128)} %copy-done.11) | copy-start | bytes 1156
  277.5 27.8 %copy-start.8 = (s32[32,3]{0,1:T(4,128)S(1)}, s32[32,3]{0,1:T(4,128)}, u32[]{:S(2)}) copy-start(s32[32,3]{0,1:T(4,128)} %param.40) | copy-start | bytes 1156
  277.6 55.7 %copy-start.9 = (f32[32,3]{0,1:T(4,128)S(1)}, f32[32,3]{0,1:T(4,128)}, u32[]{:S(2)}) copy-start(f32[32,3]{0,1:T(4,128)} %param.41) | copy-start | bytes 1156
  298.1 36.6 %copy-start.3 = (bf16[32,2048]{1,0:T(8,128)(2,1)S(1)}, bf16[32,2048]{1,0:T(8,128)(2,1)}, u32[]{:S(2)}) copy-start(bf16[32,2048]{1,0:T(8,128)(2,1)} %all-reduce.3.cloned.1.call-done) | copy-start | bytes 393220
  298.1 33.0 %all-to-all-start.2 = ((bf16[16,12,2048]{2,1,0:T(8,128)(2,1)}), bf16[16,12,2048]{2,1,0:T(8,128)(2,1)}, u32[]{:S(2)}, u32[]{:S(2)}) async-start(bf16[16,12,2048]{2,1,0:T(8,128)(2,1)} %copy.65), calls=%async_computation.3 | async-start | bytes 2097152 | tf_op jit(solution)/shard_map/all_to_all | solution.py:157
Sparse Core Ops, SparseCore 0:
  25.9 127.0 reduce-scatter.1
  155.7 49.9 all-gather.1
  208.6 17.9 all-reduce.2
  277.7 17.7 all-reduce.4
where the time goes:
time: 343 us; the launch traced here: 342 us
  waiting for transfers between devices  230 us (67%)
  blocking collectives  33.1 us (10%)
  matrix products  20.2 us (6%)
  local copies, waits for them, and re-layouts  15.4 us (4%)
  starting transfers between devices  14.5 us (4%)
  other arithmetic  14.3 us (4%)
  between operations  14 us (4%)
    reduce_scatter x1, waiting for transfers between devices, body(): lax.psum_scatter(jnp.dot(spread, joined, preferred_element_type=jnp.float...  126 us
    all_gather x1, waiting for transfers between devices, body(): lax.all_gather(w_out, 'ep', axis=1, tiled=True)  39 us
    all_to_all x1, blocking collectives, body(): lax.all_to_all(outgoing, 'ep', split_axis=0, concat_axis=0, tiled=True)  33.1 us
    all_to_all x1, waiting for transfers between devices, body(): lax.all_to_all(finished, 'ep', split_axis=0, concat_axis=0, tiled=True)  25.1 us
    psum x1, waiting for transfers between devices, body(): lax.psum(partial_out.astype(jnp.bfloat16), 'tp').astype(jnp.float32)  18.1 us
    psum x1, waiting for transfers between devices, body(): expert_sum = lax.psum(partial_down.astype(jnp.bfloat16), 'tp')  17.9 us
    all_to_all x1, starting transfers between devices, body(): lax.all_to_all(normed, 'ep', split_axis=1, concat_axis=0, tiled=True)  7.22 us
    all_to_all x1, starting transfers between devices, body(): lax.all_to_all(finished, 'ep', split_axis=0, concat_axis=0, tiled=True)  7.11 us
  transfers between devices with their start and end apart: 6, of which 6 were waited for; matrix products, arithmetic and copies ran while one was open for 5% of the time, Pallas kernels for 0%

commit v1 on v0

--- a/solution.py
+++ b/solution.py
@@ -2,6 +2,17 @@
 import jax.numpy as jnp
 from jax import lax
 from jax.sharding import PartitionSpec as P
+
+
+def in_blocks(x, dim, length):
+    before, after = (x.shape[:dim], x.shape[dim + 1 :])
+    return jnp.moveaxis(x.reshape(*before, length, -1, *after), dim, 0)
+
+
+def in_order(parts, dim):
+    lengths = list(parts.shape[1:])
+    lengths[dim] *= parts.shape[0]
+    return jnp.moveaxis(parts, 0, dim).reshape(lengths)
 
 
 def rms_scale(values_in, gain_vec):
@@ -139,7 +150,14 @@
         "rs,rd->sd", dispatch, route_rows, preferred_element_type=jnp.float32
     ).astype(jnp.bfloat16)
     outgoing = outgoing.reshape(expert_total, capacity, width)
-    received = lax.all_to_all(outgoing, "ep", split_axis=0, concat_axis=0, tiled=True)
+    size, index_2 = (lax.axis_size("ep"), lax.axis_index("ep"))
+    parts = in_blocks(outgoing, 0, size)
+    outs = [parts[index_2]]
+    for step in range(1, size):
+        sent = parts[(index_2 + step) % size]
+        outs.append(lax.ppermute(sent, "ep", [(i, (i + step) % size) for i in range(size)]))
+    parts = jnp.stack(outs)[(index_2 - jnp.arange(size)) % size]
+    received = in_order(parts, 0)
     slot_count = received.shape[1]
     regrouped = received.reshape(ep_count, local_experts, slot_count, width)
     gate_pre = jnp.einsum(

time: 343 us -> 391 us (1.14)
  waiting for transfers between devices: 230 us -> 268 us
  blocking collectives: 33.1 us -> 0 us
  starting transfers between devices: 14.5 us -> 44.2 us
  local copies, waits for them, and re-layouts: 15.4 us -> 28.6 us
    ppermute x0 -> x15, waiting for transfers between devices: none -> 33.5 us  [body(): lax.ppermute(sent, 'ep', [(i, (i + step) % size) for i in range(size)])]
    all_to_all x1 -> x0, blocking collectives: 33.1 us -> none  [body(): lax.all_to_all(outgoing, 'ep', split_axis=0, concat_axis=0, tiled=True)]
    ppermute x0 -> x15, starting transfers between devices: none -> 29.7 us  [body(): lax.ppermute(sent, 'ep', [(i, (i + step) % size) for i in range(size)])]
    unnamed x37 -> x51, local copies, waits for them, and re-layouts: 5.5 us -> 13.3 us
    psum x1, waiting for transfers between devices: 17.9 us -> 22.6 us  [body(): expert_sum = lax.psum(partial_down.astype(jnp.bfloat16), 'tp')]
  transfers between devices with their start and end apart: 6 -> 21, of which waited for: 6 -> 16; matrix products, arithmetic and copies ran while one was open for 5% -> 7% of each run, Pallas kernels for 0% -> 0%
where the time goes in v1:
time: 391 us; the launch traced here: 390 us
  waiting for transfers between devices  268 us (69%)
  starting transfers between devices  44.2 us (11%)
  local copies, waits for them, and re-layouts  28.6 us (7%)
  matrix products  20.5 us (5%)
  other arithmetic  14.8 us (4%)
  between operations  14 us (4%)
    reduce_scatter x1, waiting for transfers between devices, body(): lax.psum_scatter(jnp.dot(spread, joined, preferred_element_type=jnp.float...  126 us
    all_gather x1, waiting for transfers between devices, body(): lax.all_gather(w_out, 'ep', axis=1, tiled=True)  39 us
    ppermute x15, waiting for transfers between devices, body(): lax.ppermute(sent, 'ep', [(i, (i + step) % size) for i in range(size)])  33.5 us
    ppermute x15, starting transfers between devices, body(): lax.ppermute(sent, 'ep', [(i, (i + step) % size) for i in range(size)])  29.7 us
    all_to_all x1, waiting for transfers between devices, body(): lax.all_to_all(finished, 'ep', split_axis=0, concat_axis=0, tiled=True)  25.1 us
    psum x1, waiting for transfers between devices, body(): expert_sum = lax.psum(partial_down.astype(jnp.bfloat16), 'tp')  22.6 us
    psum x1, waiting for transfers between devices, body(): lax.psum(partial_out.astype(jnp.bfloat16), 'tp').astype(jnp.float32)  17.5 us
    unnamed x51, local copies, waits for them, and re-layouts  13.3 us
  transfers between devices with their start and end apart: 21, of which 16 were waited for; matrix products, arithmetic and copies ran while one was open for 7% of the time, Pallas kernels for 0%

profile of v1, /device:TPU:8, one launch (start us, length us, event | category | flops | bytes accessed | tf_op | source)
XLA Modules:
  0.0 390.3 jit_solution(4836763113091637783)
XLA Ops:
  7.2 1.2 fusion.36
  8.4 1.7 copy_bitcast_fusion
  10.1 7.2 %all-to-all-start = ((bf16[32,16,128]{2,0,1:T(8,128)(2,1)}), bf16[32,16,128]{2,0,1:T(8,128)(2,1)S(1)}, u32[]{:S(2)}, u32[]{:S(2)}) async-start(bf16[32,16,128]{2,0,1:T(8,128)(2,1)} %copy_bitcast_fusion), calls=%async_computation | async-start | bytes 262144 | tf_op jit(solution)/shard_map/all_to_all | solution.py:93
  19.0 1.1 concatenate.3
  20.0 3.9 all-to-all-done
  23.9 1.9 fusion.64
  27.3 125.8 %reduce-scatter.2.cloned.1.call-done = f32[32,1032]{1,0:T(8,128)} async-done(((f32[512,1032]{1,0:T(8,128)}), f32[32,1032]{1,0:T(8,128)}) %reduce-scatter.2.cloned.1.call-update) | async-done | bytes 132112 | tf_op jit(solution)/shard_map/reduce_scatter | solution.py:95
  157.0 3.7 multiply_add_fusion
  160.7 2.0 copy-done.1
  162.7 3.4 fusion.65
  166.7 39.0 %all-gather.2.cloned.1.call-done = bf16[256,2048]{1,0:T(8,128)(2,1)} async-done(((bf16[256,128]{1,0:T(8,128)(2,1)}), bf16[256,2048]{1,0:T(8,128)(2,1)}) %all-gather.2.cloned.1.call-update) | async-done | bytes 1048592 | tf_op jit(solution)/shard_map/all_gather | solution.py:127
  205.7 2.2 convolution_convert_fusion.1
  209.1 17.5 %all-reduce.3.cloned.1.call-done = bf16[32,2048]{1,0:T(8,128)(2,1)} async-done(((bf16[32,2048]{1,0:T(8,128)(2,1)}), bf16[32,2048]{1,0:T(8,128)(2,1)}) %all-reduce.3.cloned.1.call-update) | async-done | bytes 131088 | tf_op jit(solution)/shard_map/psum | solution.py:130
  226.6 1.1 fusion.40
  227.7 1.0 fusion.42
  228.9 1.1 reshape.198
  230.0 2.4 convolution_convert_fusion
  232.4 2.1 reshape_reshape.3
  234.5 2.0 dynamic-slice_bitcast_fusion
  236.5 1.5 collective-permute-start
  238.0 2.4 collective-permute-start.14
  240.9 3.3 collective-permute-start.12
  246.0 4.0 %collective-permute-done.1 = bf16[1,12,2048]{2,1,0:T(8,128)(2,1)S(1)} collective-permute-done((bf16[1,12,2048]{2,1,0:T(8,128)(2,1)S(1)}, bf16[1,12,2048]{2,1,0:T(8,128)(2,1)S(1)}, u32[]{:S(2)}, u32[]{:S(2)}) %collective-permute-start.1) | collective-permute-done | bytes 49184 | tf_op jit(solution)/shard_map/ppermute | solution.py:158
  250.0 1.5 collective-permute-start.2
  252.1 4.3 %collective-permute-done.2 = bf16[1,12,2048]{2,1,0:T(8,128)(2,1)S(1)} collective-permute-done((bf16[1,12,2048]{2,1,0:T(8,128)(2,1)S(1)}, bf16[1,12,2048]{2,1,0:T(8,128)(2,1)S(1)}, u32[]{:S(2)}, u32[]{:S(2)}) %collective-permute-start.2) | collective-permute-done | bytes 49184 | tf_op jit(solution)/shard_map/ppermute | solution.py:158
  257.3 4.3 %collective-permute-done.3 = bf16[1,12,2048]{2,1,0:T(8,128)(2,1)S(1)} collective-permute-done((bf16[1,12,2048]{2,1,0:T(8,128)(2,1)S(1)}, bf16[1,12,2048]{2,1,0:T(8,128)(2,1)S(1)}, u32[]{:S(2)}, u32[]{:S(2)}) %collective-permute-start.3) | collective-permute-done | bytes 49184 | tf_op jit(solution)/shard_map/ppermute | solution.py:158
  262.9 6.0 %collective-permute-done.4 = bf16[1,12,2048]{2,1,0:T(8,128)(2,1)S(1)} collective-permute-done((bf16[1,12,2048]{2,1,0:T(8,128)(2,1)S(1)}, bf16[1,12,2048]{2,1,0:T(8,128)(2,1)S(1)}, u32[]{:S(2)}, u32[]{:S(2)}) %collective-permute-start.4) | collective-permute-done | bytes 49184 | tf_op jit(solution)/shard_map/ppermute | solution.py:158
  269.0 1.0 collective-permute-start.5
  270.6 4.5 %collective-permute-done.5 = bf16[1,12,2048]{2,1,0:T(8,128)(2,1)S(1)} collective-permute-done((bf16[1,12,2048]{2,1,0:T(8,128)(2,1)S(1)}, bf16[1,12,2048]{2,1,0:T(8,128)(2,1)S(1)}, u32[]{:S(2)}, u32[]{:S(2)}) %collective-permute-start.5) | collective-permute-done | bytes 49184 | tf_op jit(solution)/shard_map/ppermute | solution.py:158
  275.1 4.2 %collective-permute-start.6 = (bf16[1,12,2048]{2,1,0:T(8,128)(2,1)S(1)}, bf16[1,12,2048]{2,1,0:T(8,128)(2,1)S(1)}, u32[]{:S(2)}, u32[]{:S(2)}) collective-permute-start(bf16[1,12,2048]{2,1,0:T(8,128)(2,1)S(1)} %get-tuple-element.35), channel_id=1, source_target_pairs={{0,14},{2,16},{4,18},{6,20},{8,22},{10,24},{12,26},{14,28},{16,30}... | collective-permute-start | bytes 147464 | tf_op jit(solution)/shard_map/ppermute | solution.py:158
  279.9 1.3 collective-permute-done.6
  281.2 3.9 %collective-permute-start.7 = (bf16[1,12,2048]{2,1,0:T(8,128)(2,1)S(1)}, bf16[1,12,2048]{2,1,0:T(8,128)(2,1)S(1)}, u32[]{:S(2)}, u32[]{:S(2)}) collective-permute-start(bf16[1,12,2048]{2,1,0:T(8,128)(2,1)S(1)} %get-tuple-element.34), channel_id=1, source_target_pairs={{0,16},{2,18},{4,20},{6,22},{8,24},{10,26},{12,28},{14,30},{16,0},... | collective-permute-start | bytes 147464 | tf_op jit(solution)/shard_map/ppermute | solution.py:158
  285.7 1.6 collective-permute-done.7
  287.4 3.7 collective-permute-start.8
  291.7 1.8 collective-permute-done.8
  293.4 3.4 collective-permute-start.9
  297.5 3.3 collective-permute-done.9
  300.8 2.0 collective-permute-start.10
  303.5 2.5 collective-permute-done.10
  309.1 2.8 gather_fusion
  311.9 4.1 %fusion.9 = f32[16,1,12,704]{3,0,2,1:T(8,128)} fusion(bf16[1,2048,704]{1,2,0:T(8,128)(2,1)} %param.37, bf16[16,12,2048]{2,1,0:T(8,128)(2,1)} %gather_fusion), kind=kOutput, calls=%fused_computation.12 | convolution fusion | flops 553648128 | bytes 4210688 | tf_op jit(solution)/shard_map/nxcd,xdf->nxcf/dot_general | solution.py:163
  316.0 5.2 %fusion.6 = bf16[16,12,2048]{2,0,1:T(8,128)(2,1)} fusion(bf16[1,704,2048]{2,1,0:T(8,128)(2,1)S(1)} %copy-done, bf16[1,2048,704]{1,2,0:T(8,128)(2,1)} %param.38, f32[16,1,12,704]{3,0,2,1:T(8,128)} %fusion.9, bf16[16,12,2048]{2,1,0:T(8,128)(2,1)} %gather_fusion), kind=kOutput, calls=%fused_computation.8 | convolution fusion | flops 1108500480 | bytes 7880704 | tf_op jit(solution)/shard_map/nxcf,xfd->nxcd/dot_general | solution.py:170
  321.2 22.6 %all-reduce.5.cloned.1.call-done = bf16[16,12,2048]{2,0,1:T(8,128)(2,1)} async-done(((bf16[16,12,2048]{2,0,1:T(8,128)(2,1)}), bf16[16,12,2048]{2,0,1:T(8,128)(2,1)}) %all-reduce.5.cloned.1.call-update) | async-done | bytes 786448 | tf_op jit(solution)/shard_map/psum | solution.py:173
  343.8 2.6 copy.65
  346.4 7.1 %all-to-all-start.1 = ((bf16[16,12,2048]{2,1,0:T(8,128)(2,1)}), bf16[16,12,2048]{2,1,0:T(8,128)(2,1)}, u32[]{:S(2)}, u32[]{:S(2)}) async-start(bf16[16,12,2048]{2,1,0:T(8,128)(2,1)} %copy.65), calls=%async_computation.2 | async-start | bytes 2097152 | tf_op jit(solution)/shard_map/all_to_all | solution.py:175
  354.4 25.1 %all-to-all-done.1 = bf16[16,12,2048]{2,1,0:T(8,128)(2,1)} async-done(((bf16[16,12,2048]{2,1,0:T(8,128)(2,1)}), bf16[16,12,2048]{2,1,0:T(8,128)(2,1)}, u32[]{:S(2)}, u32[]{:S(2)}) %all-to-all-start.1) | async-done | bytes 786464 | tf_op jit(solution)/shard_map/all_to_all | solution.py:175
  379.4 2.1 reshape.225
  381.6 1.5 fusion.18
  (99 shorter events, 22.7 us)
Async XLA Ops:
  7.2 308.9 %copy-start = (bf16[1,704,2048]{2,1,0:T(8,128)(2,1)S(1)}, bf16[1,704,2048]{2,1,0:T(8,128)(2,1)}, u32[]{:S(2)}) copy-start(bf16[1,704,2048]{2,1,0:T(8,128)(2,1)} %param.39) | copy-start | bytes 8650756
  10.1 13.8 %all-to-all-start = ((bf16[32,16,128]{2,0,1:T(8,128)(2,1)}), bf16[32,16,128]{2,0,1:T(8,128)(2,1)S(1)}, u32[]{:S(2)}, u32[]{:S(2)}) async-start(bf16[32,16,128]{2,0,1:T(8,128)(2,1)} %copy_bitcast_fusion), calls=%async_computation | async-start | bytes 262144 | tf_op jit(solution)/shard_map/all_to_all | solution.py:93
  17.3 135.8 %reduce-scatter.2.cloned.1.call-start = ((), (), s32[]{:S(2)}) async-start(), calls=%async_computation.3 | async-start | bytes 2506752 | tf_op jit(solution)/shard_map/reduce_scatter | solution.py:95
  18.9 7.6 %copy-start.12 = (f32[32,4]{0,1:T(4,128)S(1)}, f32[32,4]{0,1:T(4,128)}, u32[]{:S(2)}) copy-start(f32[32,4]{0,1:T(4,128)} %param.35) | copy-start | bytes 1540
  18.9 7.7 %copy-start.6 = (s32[32,3]{0,1:T(4,128)S(1)}, s32[32,3]{0,1:T(4,128)}, u32[]{:S(2)}) copy-start(s32[32,3]{0,1:T(4,128)} %param.40) | copy-start | bytes 1156
  23.9 130.5 %copy-start.9 = (f32[4]{0:T(128)S(1)}, f32[4]{0:T(128)}, u32[]{:S(2)}) copy-start(f32[4]{0:T(128)} %param.30) | copy-start | bytes 52
  23.9 130.5 %copy-start.14 = (f32[4]{0:T(128)S(1)}, f32[4]{0:T(128)}, u32[]{:S(2)}) copy-start(f32[4]{0:T(128)} %param.29) | copy-start | bytes 52
  23.9 132.3 %copy-start.4 = (f32[32,4,64]{2,1,0:T(4,128)S(1)}, f32[32,4,64]{2,1,0:T(4,128)}, u32[]{:S(2)}) copy-start(f32[32,4,64]{2,1,0:T(4,128)} %param.34) | copy-start | bytes 98308
  25.8 180.0 %all-gather.2.cloned.1.call-start = ((), (), s32[]{:S(2)}) async-start(), calls=%async_computation.4 | async-start | bytes 1114112 | tf_op jit(solution)/shard_map/all_gather | solution.py:127
  26.5 200.1 %all-reduce.3.cloned.1.call-start = ((), (), s32[]{:S(2)}) async-start(), calls=%async_computation.5 | async-start | bytes 262144 | tf_op jit(solution)/shard_map/psum | solution.py:130
  27.3 180.7 %copy-start.10 = (s32[96]{0:T(128)}, s32[96]{0:T(128)S(1)}, u32[]{:S(2)}) copy-start(s32[96]{0:T(128)S(1)} %select_reduce_fusion) | copy-start | bytes 1156
  160.7 2.0 copy-start.1
  162.7 43.0 %copy-start.13 = (f32[256]{0:T(256)S(1)}, f32[256]{0:T(256)}, u32[]{:S(2)}) copy-start(f32[256]{0:T(256)} %param.31) | copy-start | bytes 3076
  162.7 63.9 %copy-start.2 = (bf16[32,2048]{1,0:T(8,128)(2,1)S(1)}, bf16[32,2048]{1,0:T(8,128)(2,1)}, u32[]{:S(2)}) copy-start(bf16[32,2048]{1,0:T(8,128)(2,1)} %param.21) | copy-start | bytes 393220
  162.7 64.9 %copy-start.5 = (f32[2048]{0:T(1024)S(1)}, f32[2048]{0:T(1024)}, u32[]{:S(2)}) copy-start(f32[2048]{0:T(1024)} %param.36) | copy-start | bytes 24580
  207.9 135.9 %all-reduce.5.cloned.1.call-start = ((), (), s32[]{:S(2)}) async-start(), calls=%async_computation.6 | async-start | bytes 1572864 | tf_op jit(solution)/shard_map/psum | solution.py:173
  230.0 8.0 %copy-start.15 = (s32[16]{0:T(128)S(1)}, s32[16]{0:T(128)}, u32[]{:S(2)}) copy-start(s32[16]{0:T(128)} %fusion.58) | copy-start | bytes 196
  236.5 8.3 %collective-permute-start = (bf16[1,12,2048]{2,1,0:T(8,128)(2,1)S(1)}, bf16[1,12,2048]{2,1,0:T(8,128)(2,1)S(1)}, u32[]{:S(2)}, u32[]{:S(2)}) collective-permute-start(bf16[1,12,2048]{2,1,0:T(8,128)(2,1)S(1)} %get-tuple-element.41), channel_id=1, source_target_pairs={{0,2},{2,4},{4,6},{6,8},{8,10},{10,12},{12,14},{14,16},{16,18},{18... | collective-permute-start | bytes 147464 | tf_op jit(solution)/shard_map/ppermute | solution.py:158
  238.0 70.5 %collective-permute-start.14 = (bf16[1,12,2048]{2,1,0:T(8,128)(2,1)S(1)}, bf16[1,12,2048]{2,1,0:T(8,128)(2,1)S(1)}, u32[]{:S(2)}, u32[]{:S(2)}) collective-permute-start(bf16[1,12,2048]{2,1,0:T(8,128)(2,1)S(1)} %get-tuple-element.27), channel_id=1, source_target_pairs={{0,30},{2,0},{4,2},{6,4},{8,6},{10,8},{12,10},{14,12},{16,14},{18,... | collective-permute-start | bytes 147464 | tf_op jit(solution)/shard_map/ppermute | solution.py:158
  240.4 67.5 %collective-permute-start.13 = (bf16[1,12,2048]{2,1,0:T(8,128)(2,1)S(1)}, bf16[1,12,2048]{2,1,0:T(8,128)(2,1)S(1)}, u32[]{:S(2)}, u32[]{:S(2)}) collective-permute-start(bf16[1,12,2048]{2,1,0:T(8,128)(2,1)S(1)} %get-tuple-element.28), channel_id=1, source_target_pairs={{0,28},{2,30},{4,0},{6,2},{8,4},{10,6},{12,8},{14,10},{16,12},{18,... | collective-permute-start | bytes 147464 | tf_op jit(solution)/shard_map/ppermute | solution.py:158
  240.9 66.3 %collective-permute-start.12 = (bf16[1,12,2048]{2,1,0:T(8,128)(2,1)S(1)}, bf16[1,12,2048]{2,1,0:T(8,128)(2,1)S(1)}, u32[]{:S(2)}, u32[]{:S(2)}) collective-permute-start(bf16[1,12,2048]{2,1,0:T(8,128)(2,1)S(1)} %get-tuple-element.29), channel_id=1, source_target_pairs={{0,26},{2,28},{4,30},{6,0},{8,2},{10,4},{12,6},{14,8},{16,10},{18,... | collective-permute-start | bytes 147464 | tf_op jit(solution)/shard_map/ppermute | solution.py:158
  244.3 62.3 %collective-permute-start.11 = (bf16[1,12,2048]{2,1,0:T(8,128)(2,1)S(1)}, bf16[1,12,2048]{2,1,0:T(8,128)(2,1)S(1)}, u32[]{:S(2)}, u32[]{:S(2)}) collective-permute-start(bf16[1,12,2048]{2,1,0:T(8,128)(2,1)S(1)} %get-tuple-element.30), channel_id=1, source_target_pairs={{0,24},{2,26},{4,28},{6,30},{8,0},{10,2},{12,4},{14,6},{16,8},{18,... | collective-permute-start | bytes 147464 | tf_op jit(solution)/shard_map/ppermute | solution.py:158
  244.8 5.2 %collective-permute-start.1 = (bf16[1,12,2048]{2,1,0:T(8,128)(2,1)S(1)}, bf16[1,12,2048]{2,1,0:T(8,128)(2,1)S(1)}, u32[]{:S(2)}, u32[]{:S(2)}) collective-permute-start(bf16[1,12,2048]{2,1,0:T(8,128)(2,1)S(1)} %get-tuple-element.40), channel_id=1, source_target_pairs={{0,4},{2,6},{4,8},{6,10},{8,12},{10,14},{12,16},{14,18},{16,20},{1... | collective-permute-start | bytes 147464 | tf_op jit(solution)/shard_map/ppermute | solution.py:158
  250.0 6.4 %collective-permute-start.2 = (bf16[1,12,2048]{2,1,0:T(8,128)(2,1)S(1)}, bf16[1,12,2048]{2,1,0:T(8,128)(2,1)S(1)}, u32[]{:S(2)}, u32[]{:S(2)}) collective-permute-start(bf16[1,12,2048]{2,1,0:T(8,128)(2,1)S(1)} %get-tuple-element.39), channel_id=1, source_target_pairs={{0,6},{2,8},{4,10},{6,12},{8,14},{10,16},{12,18},{14,20},{16,22},{... | collective-permute-start | bytes 147464 | tf_op jit(solution)/shard_map/ppermute | solution.py:158
  256.4 5.2 %collective-permute-start.3 = (bf16[1,12,2048]{2,1,0:T(8,128)(2,1)S(1)}, bf16[1,12,2048]{2,1,0:T(8,128)(2,1)S(1)}, u32[]{:S(2)}, u32[]{:S(2)}) collective-permute-start(bf16[1,12,2048]{2,1,0:T(8,128)(2,1)S(1)} %get-tuple-element.38), channel_id=1, source_target_pairs={{0,8},{2,10},{4,12},{6,14},{8,16},{10,18},{12,20},{14,22},{16,24},... | collective-permute-start | bytes 147464 | tf_op jit(solution)/shard_map/ppermute | solution.py:158
  261.5 7.5 %collective-permute-start.4 = (bf16[1,12,2048]{2,1,0:T(8,128)(2,1)S(1)}, bf16[1,12,2048]{2,1,0:T(8,128)(2,1)S(1)}, u32[]{:S(2)}, u32[]{:S(2)}) collective-permute-start(bf16[1,12,2048]{2,1,0:T(8,128)(2,1)S(1)} %get-tuple-element.37), channel_id=1, source_target_pairs={{0,10},{2,12},{4,14},{6,16},{8,18},{10,20},{12,22},{14,24},{16,26}... | collective-permute-start | bytes 147464 | tf_op jit(solution)/shard_map/ppermute | solution.py:158
  269.0 6.1 %collective-permute-start.5 = (bf16[1,12,2048]{2,1,0:T(8,128)(2,1)S(1)}, bf16[1,12,2048]{2,1,0:T(8,128)(2,1)S(1)}, u32[]{:S(2)}, u32[]{:S(2)}) collective-permute-start(bf16[1,12,2048]{2,1,0:T(8,128)(2,1)S(1)} %get-tuple-element.36), channel_id=1, source_target_pairs={{0,12},{2,14},{4,16},{6,18},{8,20},{10,22},{12,24},{14,26},{16,28}... | collective-permute-start | bytes 147464 | tf_op jit(solution)/shard_map/ppermute | solution.py:158
  275.1 6.1 %collective-permute-start.6 = (bf16[1,12,2048]{2,1,0:T(8,128)(2,1)S(1)}, bf16[1,12,2048]{2,1,0:T(8,128)(2,1)S(1)}, u32[]{:S(2)}, u32[]{:S(2)}) collective-permute-start(bf16[1,12,2048]{2,1,0:T(8,128)(2,1)S(1)} %get-tuple-element.35), channel_id=1, source_target_pairs={{0,14},{2,16},{4,18},{6,20},{8,22},{10,24},{12,26},{14,28},{16,30}... | collective-permute-start | bytes 147464 | tf_op jit(solution)/shard_map/ppermute | solution.py:158
  281.2 6.2 %collective-permute-start.7 = (bf16[1,12,2048]{2,1,0:T(8,128)(2,1)S(1)}, bf16[1,12,2048]{2,1,0:T(8,128)(2,1)S(1)}, u32[]{:S(2)}, u32[]{:S(2)}) collective-permute-start(bf16[1,12,2048]{2,1,0:T(8,128)(2,1)S(1)} %get-tuple-element.34), channel_id=1, source_target_pairs={{0,16},{2,18},{4,20},{6,22},{8,24},{10,26},{12,28},{14,30},{16,0},... | collective-permute-start | bytes 147464 | tf_op jit(solution)/shard_map/ppermute | solution.py:158
  287.4 6.1 %collective-permute-start.8 = (bf16[1,12,2048]{2,1,0:T(8,128)(2,1)S(1)}, bf16[1,12,2048]{2,1,0:T(8,128)(2,1)S(1)}, u32[]{:S(2)}, u32[]{:S(2)}) collective-permute-start(bf16[1,12,2048]{2,1,0:T(8,128)(2,1)S(1)} %get-tuple-element.33), channel_id=1, source_target_pairs={{0,18},{2,20},{4,22},{6,24},{8,26},{10,28},{12,30},{14,0},{16,2},{... | collective-permute-start | bytes 147464 | tf_op jit(solution)/shard_map/ppermute | solution.py:158
  293.4 7.4 %collective-permute-start.9 = (bf16[1,12,2048]{2,1,0:T(8,128)(2,1)S(1)}, bf16[1,12,2048]{2,1,0:T(8,128)(2,1)S(1)}, u32[]{:S(2)}, u32[]{:S(2)}) collective-permute-start(bf16[1,12,2048]{2,1,0:T(8,128)(2,1)S(1)} %get-tuple-element.32), channel_id=1, source_target_pairs={{0,20},{2,22},{4,24},{6,26},{8,28},{10,30},{12,0},{14,2},{16,4},{1... | collective-permute-start | bytes 147464 | tf_op jit(solution)/shard_map/ppermute | solution.py:158
  300.8 5.2 %collective-permute-start.10 = (bf16[1,12,2048]{2,1,0:T(8,128)(2,1)S(1)}, bf16[1,12,2048]{2,1,0:T(8,128)(2,1)S(1)}, u32[]{:S(2)}, u32[]{:S(2)}) collective-permute-start(bf16[1,12,2048]{2,1,0:T(8,128)(2,1)S(1)} %get-tuple-element.31), channel_id=1, source_target_pairs={{0,22},{2,24},{4,26},{6,28},{8,30},{10,0},{12,2},{14,4},{16,6},{18... | collective-permute-start | bytes 147464 | tf_op jit(solution)/shard_map/ppermute | solution.py:158
  321.2 32.3 %copy-start.11 = (s32[96]{0:T(128)S(1)}, s32[96]{0:T(128)}, u32[]{:S(2)}) copy-start(s32[96]{0:T(128)} %copy-done.10) | copy-start | bytes 1156
  321.2 32.5 %copy-start.7 = (s32[32,3]{0,1:T(4,128)S(1)}, s32[32,3]{0,1:T(4,128)}, u32[]{:S(2)}) copy-start(s32[32,3]{0,1:T(4,128)} %param.40) | copy-start | bytes 1156
  321.2 60.3 %copy-start.8 = (f32[32,3]{0,1:T(4,128)S(1)}, f32[32,3]{0,1:T(4,128)}, u32[]{:S(2)}) copy-start(f32[32,3]{0,1:T(4,128)} %param.41) | copy-start | bytes 1156
  346.4 36.6 %copy-start.3 = (bf16[32,2048]{1,0:T(8,128)(2,1)S(1)}, bf16[32,2048]{1,0:T(8,128)(2,1)}, u32[]{:S(2)}) copy-start(bf16[32,2048]{1,0:T(8,128)(2,1)} %all-reduce.3.cloned.1.call-done) | copy-start | bytes 393220
  346.4 33.0 %all-to-all-start.1 = ((bf16[16,12,2048]{2,1,0:T(8,128)(2,1)}), bf16[16,12,2048]{2,1,0:T(8,128)(2,1)}, u32[]{:S(2)}, u32[]{:S(2)}) async-start(bf16[16,12,2048]{2,1,0:T(8,128)(2,1)} %copy.65), calls=%async_computation.2 | async-start | bytes 2097152 | tf_op jit(solution)/shard_map/all_to_all | solution.py:175
Sparse Core Ops, SparseCore 0:
  25.9 127.1 reduce-scatter.1
  155.8 49.9 all-gather.1
  208.6 17.9 all-reduce.2
  321.3 22.4 all-reduce.4
